TPU v7x, 256 devices: a 4x2x16 block of a 4x16x16 slice. The times are simulated.
256 devices in a mesh: grp: 2 (over y), sp: 16 (over z), tp: 8 (over x, core).
Axes of the slice: x: 4, y: 2, z: 16, core: 2. Of those that a mesh axis runs over, the one named last changes fastest.
The devices are a block of a 4x16x16 slice.
Arguments:
- queries: bfloat16 [24576, 1024], P(('grp', 'sp'), 'tp'), parts along dimension 0, may hold values from -200 to 200
- key_rows: bfloat16 [24576, 512], P(('grp', 'sp'), 'tp'), parts along dimension 0, may hold values from -6 to 6
- value_rows: bfloat16 [24576, 512], P(('grp', 'sp'), 'tp'), parts along dimension 0, may hold values from -6 to 6
- doc_ids: int32 [24576], P(('grp', 'sp')), parts along dimension 0, may hold values from 0 to 7, never falling along the last dimension, each value on 1 to 3072 neighbouring positions
- sink_logits: float32 [16], P('tp'), may hold values from 2 to 7
- out_weight: bfloat16 [1024, 2048], P('tp', 'sp'), may hold values from -0.1875 to 0.1875
- residual: bfloat16 [24576, 2048], P(('grp', 'sp', 'tp')), parts along dimension 0, may hold values from -6 to 6
- gain_mixed: float32 [2048], replicated, may hold values from 0.1 to 1.9
- gain_before: float32 [2048], replicated, may hold values from 0.1 to 1.9
- gain_after: float32 [2048], replicated, may hold values from 0.1 to 1.9
- gate_weight: bfloat16 [2048, 6144], P('sp', 'tp'), may hold values from -0.125 to 0.125
- up_weight: bfloat16 [2048, 6144], P('sp', 'tp'), may hold values from -0.125 to 0.125
- down_weight: bfloat16 [6144, 2048], P('tp', 'sp'), may hold values from -0.078125 to 0.078125
Outputs:
- layer_out: bfloat16 [24576, 2048], P(('grp', 'sp', 'tp')), parts along dimension 0
There are 2 independent parts, one for each index of `grp`. A program takes and returns all parts, laid end to end along the dimension named above; an argument that names none is the same for every part. Nothing has to cross between parts.
All inputs are finite; a program needn't handle non-finite values.
Results may differ from a plain program's by a relative error of at most 0.015.
Values may be sent and summed in bfloat16 or wider, within the bound.
A program may use at most 128 MiB of HBM per device.

v0:
```python
import jax
import jax.numpy as jnp
from jax import lax
from jax.sharding import PartitionSpec as P

HEAD_DIM = 64
WINDOW = 128
epsilon = 1e-06
masked_value = -1e30


def passed_along(value, axis, steps):
    count = lax.axis_size(axis)
    first, last = (max(0, -steps), min(count, count - steps))
    return lax.ppermute(value, axis, [(source, source + steps) for source in range(first, last)])


def from_everyone(shard, axis):
    size = lax.axis_size(axis)
    return lax.all_to_all(
        jnp.broadcast_to(shard[None], (size, *shard.shape)), axis, 0, 0, tiled=True
    )


def laid_out(pieces, dim):
    pieces = jnp.moveaxis(pieces, 0, dim)
    lengths = pieces.shape
    return pieces.reshape(*lengths[:dim], lengths[dim] * lengths[dim + 1], *lengths[dim + 2 :])


def gather_directly(shard, axis, dim):
    pieces = from_everyone(shard, axis)
    return laid_out(pieces, dim)


def turned_gather(arrays, axis, dims):
    turned = [jnp.moveaxis(a, dim, 0) for a, dim in zip(arrays, dims)]
    both = jnp.concatenate([t.reshape(len(t), -1) for t in turned], axis=1)
    filled, at, finished = (lax.all_gather(both, axis, axis=0, tiled=True), 0, [])
    for t, dim in zip(turned, dims):
        piece = filled[:, at : at + t[0].size].reshape(-1, *t.shape[1:])
        finished.append(jnp.moveaxis(piece, 0, dim))
        at += t[0].size
    return tuple(finished)


def split_up(shard, dim, size):
    lengths = shard.shape
    pieces = shard.reshape(*lengths[:dim], size, lengths[dim] // size, *lengths[dim + 1 :])
    return jnp.moveaxis(pieces, dim, 0)


def summed_on_arrival(shard, axis, dim):
    size = lax.axis_size(axis)
    pieces = lax.all_to_all(split_up(shard, dim, size), axis, 0, 0, tiled=True)
    return jnp.sum(pieces.astype(jnp.float32), axis=0)


def stored(value):
    return lax.optimization_barrier(value.astype(jnp.bfloat16)).astype(jnp.float32)


def rms_scaled(value, gain):
    return value * lax.rsqrt(jnp.mean(value * value, axis=-1, keepdims=True) + epsilon) * gain


def windows(array, blocks):
    first = array[:-WINDOW].reshape((blocks, WINDOW) + array.shape[1:])
    second = array[WINDOW:].reshape((blocks, WINDOW) + array.shape[1:])
    return jnp.concatenate([first, second], axis=1)


def attend(queries, key_rows, value_rows, doc_ids, sink_logits):
    length = queries.shape[0]
    blocks = length // WINDOW
    local_kv = key_rows.shape[1] // HEAD_DIM
    group_size = queries.shape[1] // HEAD_DIM // local_kv
    offset = lax.axis_index("sp") * length
    tail_keys, tail_values, tail_docs = passed_along(
        (key_rows[length - WINDOW :], value_rows[length - WINDOW :], doc_ids[length - WINDOW :]),
        "sp",
        1,
    )
    key_blocks = windows(jnp.concatenate([tail_keys, key_rows], axis=0), blocks).reshape(
        blocks, 2 * WINDOW, local_kv, HEAD_DIM
    )
    value_blocks = windows(jnp.concatenate([tail_values, value_rows], axis=0), blocks).reshape(
        blocks, 2 * WINDOW, local_kv, HEAD_DIM
    )
    key_docs = windows(jnp.concatenate([tail_docs, doc_ids], axis=0), blocks)
    key_places = windows(offset - WINDOW + jnp.arange(length + WINDOW, dtype=jnp.int32), blocks)
    query_places = (offset + jnp.arange(length, dtype=jnp.int32)).reshape(blocks, WINDOW)
    query_docs = doc_ids.reshape(blocks, WINDOW)
    query_blocks = queries.reshape(blocks, WINDOW, local_kv, group_size, HEAD_DIM)
    scores = jnp.einsum(
        "bqhgd,bkhd->bhgqk", query_blocks, key_blocks, preferred_element_type=jnp.float32
    ) * HEAD_DIM ** (-0.5)
    distance = query_places[:, :, None] - key_places[:, None, :]
    valid = (distance >= 0) & (distance < WINDOW) & (key_places[:, None, :] >= 0)
    valid = valid & (query_docs[:, :, None] == key_docs[:, None, :])
    scores = jnp.where(valid[:, None, None], scores, masked_value)
    sinks = sink_logits.reshape(local_kv, group_size)[None, :, :, None]
    top = jnp.maximum(jnp.max(scores, axis=-1), sinks)
    weight = jnp.exp(scores - top[..., None])
    denom = jnp.sum(weight, axis=-1) + jnp.exp(sinks - top)
    summed = jnp.einsum(
        "bhgqk,bkhd->bqhgd",
        weight.astype(jnp.bfloat16),
        value_blocks,
        preferred_element_type=jnp.float32,
    )
    scale = jnp.transpose(denom, (0, 3, 1, 2))[..., None]
    return (summed / scale).reshape(length, queries.shape[1]).astype(jnp.bfloat16)


def per_device(
    queries,
    key_rows,
    value_rows,
    doc_ids,
    sink_logits,
    out_weight,
    residual,
    gain_mixed,
    gain_before,
    gain_after,
    gate_weight,
    up_weight,
    down_weight,
):
    mixed = attend(queries, key_rows, value_rows, doc_ids, sink_logits)
    head_columns = gather_directly(out_weight, "sp", 1)
    by_rows = lax.all_to_all(mixed, "tp", split_axis=0, concat_axis=1, tiled=True)
    projected = jnp.dot(
        by_rows,
        lax.all_gather(head_columns, "tp", axis=0, tiled=True),
        preferred_element_type=jnp.float32,
    )
    projected = stored(projected)
    after = stored(residual.astype(jnp.float32) + rms_scaled(projected, gain_mixed))
    normed = rms_scaled(after, gain_before).astype(jnp.bfloat16)
    full_gate, full_up, full_down = turned_gather(
        (gate_weight, up_weight, down_weight), "sp", (0, 0, 1)
    )
    piece = lax.all_gather(normed, "tp", axis=0, tiled=True)
    gate = jnp.dot(piece, full_gate, preferred_element_type=jnp.float32)
    upward = jnp.dot(piece, full_up, preferred_element_type=jnp.float32)
    hidden = (jax.nn.silu(gate) * upward).astype(jnp.bfloat16)
    ffn_out = stored(
        summed_on_arrival(
            jnp.dot(hidden, full_down, preferred_element_type=jnp.float32).astype(jnp.bfloat16),
            "tp",
            0,
        )
    )
    return (after + 0.5 * rms_scaled(ffn_out, gain_after)).astype(jnp.bfloat16)


def solution(mesh):
    return jax.shard_map(
        per_device,
        mesh=mesh,
        in_specs=(
            P(("grp", "sp"), "tp"),
            P(("grp", "sp"), "tp"),
            P(("grp", "sp"), "tp"),
            P(("grp", "sp")),
            P("tp"),
            P("tp", "sp"),
            P(("grp", "sp", "tp"), None),
            P(),
            P(),
            P(),
            P("sp", "tp"),
            P("sp", "tp"),
            P("tp", "sp"),
        ),
        out_specs=P(("grp", "sp", "tp"), None),
        check_vma=False,
    )
```

profile of v0, /device:TPU:33, one launch (start us, length us, event | category | flops | bytes accessed | tf_op | source)
XLA Modules:
  0.0 348.9 jit_solution(4281266326615611289)
XLA Ops:
  6.6 1.0 copy.40
  7.7 47.2 %all_to_all.26 = bf16[16,128,128]{1,2,0:T(8,128)(2,1)} all-to-all(bf16[16,128,128]{1,2,0:T(8,128)(2,1)S(1)} %broadcast_in_dim.16), channel_id=1, replica_groups=mesh['grp'=2,'sp'=16,'tp'=8] {'sp'}, dimensions={0} | all-to-all | bytes 1048576 | tf_op jit(solution)/shard_map/all_to_all | solution.py:20
  55.0 0.7 slice.49
  55.7 5.3 %collective-permute-start.1 = (s32[128]{0:T(128)S(1)}, s32[128]{0:T(128)S(1)}, u32[]{:S(2)}, u32[]{:S(2)}) collective-permute-start(s32[128]{0:T(128)S(1)} %slice.49), channel_id=1, source_target_pairs={{0,8},{8,16},{16,24},{24,32},{32,40},{40,48},{48,56},{56,64},{64,7... | collective-permute-start | bytes 1544 | tf_op jit(solution)/shard_map/ppermute | solution.py:15
  61.0 0.7 slice.45
  61.7 2.2 collective-permute-start
  63.9 0.7 slice.52
  64.6 4.6 %collective-permute-start.2 = (bf16[128,64]{0,1:T(8,128)(2,1)S(1)}, bf16[128,64]{0,1:T(8,128)(2,1)S(1)}, u32[]{:S(2)}, u32[]{:S(2)}) collective-permute-start(bf16[128,64]{0,1:T(8,128)(2,1)S(1)} %slice.52), channel_id=1, source_target_pairs={{0,8},{8,16},{16,24},{24,32},{32,40},{40,48},{48,56},{56,64},{64,7... | collective-permute-start | bytes 49160 | tf_op jit(solution)/shard_map/ppermute | solution.py:15
  69.6 1.0 fusion.30
  70.6 0.5 fusion.48
  71.9 0.4 copy.48
  72.5 17.5 %all_to_all.27 = bf16[8,96,128]{2,1,0:T(8,128)(2,1)S(1)} all-to-all(bf16[8,96,128]{2,1,0:T(8,128)(2,1)S(1)} %reshape.171), channel_id=1, replica_groups=mesh['grp'=2,'sp'=16,'tp'=8] {'tp'}, dimensions={0} | all-to-all | bytes 393216 | tf_op jit(solution)/shard_map/all_to_all | solution.py:133
  90.0 12.1 %all-gather.4.cloned.1.call-done = bf16[1024,2048]{0,1:T(8,128)(2,1)} async-done(((bf16[128,2048]{0,1:T(8,128)(2,1)}), bf16[1024,2048]{0,1:T(8,128)(2,1)}) %all-gather.4.cloned.1.call-update) | async-done | bytes 4194320 | tf_op jit(solution)/shard_map/all_gather | solution.py:136
  102.2 3.6 %convolution_convert_fusion.1 = bf16[96,2048]{1,0:T(8,128)(2,1)S(1)} fusion(bf16[1024,2048]{0,1:T(8,128)(2,1)} %all-gather.4.cloned.1.call-done, bf16[8,96,128]{2,1,0:T(8,128)(2,1)S(1)} %all_to_all.27), kind=kOutput, calls=%fused_computation.7 | convolution fusion | flops 402849792 | bytes 4784128 | tf_op jit(solution)/shard_map/dot_general | solution.py:134
  106.4 0.9 fusion.23
  108.0 0.9 pad_maximum_fusion
  108.9 31.3 %all-gather.6.cloned.1.call-done = bf16[768,2048]{1,0:T(8,128)(2,1)} async-done(((bf16[96,2048]{1,0:T(8,128)(2,1)}), bf16[768,2048]{1,0:T(8,128)(2,1)}) %all-gather.6.cloned.1.call-update) | async-done | bytes 3145744 | tf_op jit(solution)/shard_map/all_gather | solution.py:145
  140.2 128.3 %all-gather.8.cloned.1.call-done = bf16[2048,2304]{0,1:T(8,128)(2,1)} async-done(((bf16[128,2304]{0,1:T(8,128)(2,1)}), bf16[2048,2304]{0,1:T(8,128)(2,1)}) %all-gather.8.cloned.1.call-update) | async-done | bytes 9437200 | tf_op jit(solution)/shard_map/all_gather | solution.py:39
  268.5 6.9 %fusion.3 = f32[768,768]{1,0:T(8,128)} fusion(bf16[768,2048]{1,0:T(8,128)(2,1)} %all-gather.6.cloned.1.call-done, bf16[2048,2304]{0,1:T(8,128)(2,1)} %all-gather.8.cloned.1.call-done), kind=kOutput, calls=%fused_computation.4 | convolution fusion | flops 2415919104 | bytes 8650752 | tf_op jit(solution)/shard_map/dot_general | solution.py:146
  275.4 11.0 %convolution_convert_fusion = bf16[768,2048]{1,0:T(8,128)(2,1)} fusion(bf16[2048,2304]{0,1:T(8,128)(2,1)} %all-gather.8.cloned.1.call-done, f32[768,768]{1,0:T(8,128)} %fusion.3, bf16[768,2048]{1,0:T(8,128)(2,1)S(1)} %copy-done.12), kind=kOutput, calls=%fused_computation | convolution fusion | flops 4836950016 | bytes 14942208 | tf_op jit(solution)/shard_map/dot_general | solution.py:151
  286.4 51.4 %all_to_all.28 = bf16[8,96,2048]{2,1,0:T(8,128)(2,1)S(1)} all-to-all(bf16[8,96,2048]{2,1,0:T(8,128)(2,1)} %bitcast.84), channel_id=1, replica_groups=mesh['grp'=2,'sp'=16,'tp'=8] {'tp'}, dimensions={0} | all-to-all | bytes 6291456 | tf_op jit(solution)/shard_map/all_to_all | solution.py:55
  337.7 1.4 reduce_sum.54
  339.2 1.2 fusion.18
  340.4 2.0 fusion.24
  (61 shorter events, 2.8 us)
Async XLA Ops:
  6.5 63.0 %copy-start.7 = (s32[768]{0:T(1024)S(1)}, s32[768]{0:T(1024)}, u32[]{:S(2)}) copy-start(s32[768]{0:T(1024)} %param.16) | copy-start | bytes 9220
  6.5 62.7 %copy-start.1 = (bf16[768,64]{0,1:T(8,128)(2,1)S(1)}, bf16[768,64]{0,1:T(8,128)(2,1)}, u32[]{:S(2)}) copy-start(bf16[768,64]{0,1:T(8,128)(2,1)} %param.15) | copy-start | bytes 294916
  6.6 62.7 %copy-start = (bf16[768,64]{0,1:T(8,128)(2,1)S(1)}, bf16[768,64]{0,1:T(8,128)(2,1)}, u32[]{:S(2)}) copy-start(bf16[768,64]{0,1:T(8,128)(2,1)} %param.14) | copy-start | bytes 294916
  6.6 62.8 %copy-start.6 = (bf16[768,128]{1,0:T(8,128)(2,1)S(1)}, bf16[768,128]{1,0:T(8,128)(2,1)}, u32[]{:S(2)}) copy-start(bf16[768,128]{1,0:T(8,128)(2,1)} %param.13) | copy-start | bytes 589828
  6.6 95.6 %all-gather.4.cloned.1.call-start = ((), (), s32[]{:S(2)}) async-start(), calls=%async_computation.3 | async-start | bytes 4718592 | tf_op jit(solution)/shard_map/all_gather | solution.py:136
  54.9 16.2 %copy-start.11 = (f32[2]{0:T(128)S(1)}, f32[2]{0:T(128)}, u32[]{:S(2)}) copy-start(f32[2]{0:T(128)} %param.17) | copy-start | bytes 28
  54.9 85.2 %all-gather.6.cloned.1.call-start = ((), (), s32[]{:S(2)}) async-start(), calls=%async_computation.4 | async-start | bytes 3538944 | tf_op jit(solution)/shard_map/all_gather | solution.py:145
  55.7 13.8 %collective-permute-start.1 = (s32[128]{0:T(128)S(1)}, s32[128]{0:T(128)S(1)}, u32[]{:S(2)}, u32[]{:S(2)}) collective-permute-start(s32[128]{0:T(128)S(1)} %slice.49), channel_id=1, source_target_pairs={{0,8},{8,16},{16,24},{24,32},{32,40},{40,48},{48,56},{56,64},{64,7... | collective-permute-start | bytes 1544 | tf_op jit(solution)/shard_map/ppermute | solution.py:15
  61.7 8.9 %collective-permute-start = (bf16[128,64]{0,1:T(8,128)(2,1)S(1)}, bf16[128,64]{0,1:T(8,128)(2,1)S(1)}, u32[]{:S(2)}, u32[]{:S(2)}) collective-permute-start(bf16[128,64]{0,1:T(8,128)(2,1)S(1)} %slice.45), channel_id=1, source_target_pairs={{0,8},{8,16},{16,24},{24,32},{32,40},{40,48},{48,56},{56,64},{64,7... | collective-permute-start | bytes 49160 | tf_op jit(solution)/shard_map/ppermute | solution.py:15
  64.6 5.9 %collective-permute-start.2 = (bf16[128,64]{0,1:T(8,128)(2,1)S(1)}, bf16[128,64]{0,1:T(8,128)(2,1)S(1)}, u32[]{:S(2)}, u32[]{:S(2)}) collective-permute-start(bf16[128,64]{0,1:T(8,128)(2,1)S(1)} %slice.52), channel_id=1, source_target_pairs={{0,8},{8,16},{16,24},{24,32},{32,40},{40,48},{48,56},{56,64},{64,7... | collective-permute-start | bytes 49160 | tf_op jit(solution)/shard_map/ppermute | solution.py:15
  90.0 16.0 %copy-start.2 = (bf16[96,2048]{1,0:T(8,128)(2,1)S(1)}, bf16[96,2048]{1,0:T(8,128)(2,1)}, u32[]{:S(2)}) copy-start(bf16[96,2048]{1,0:T(8,128)(2,1)} %param.19) | copy-start | bytes 1179652
  90.0 16.0 %copy-start.8 = (f32[2048]{0:T(1024)S(1)}, f32[2048]{0:T(1024)}, u32[]{:S(2)}) copy-start(f32[2048]{0:T(1024)} %param.20) | copy-start | bytes 24580
  90.0 16.4 %copy-start.9 = (f32[2048]{0:T(1024)S(1)}, f32[2048]{0:T(1024)}, u32[]{:S(2)}) copy-start(f32[2048]{0:T(1024)} %param.21) | copy-start | bytes 24580
  105.8 1.9 copy-start.4
  105.8 2.0 copy-start.5
  105.8 2.2 copy-start.3
  107.4 161.1 %all-gather.8.cloned.1.call-start = ((), (), s32[]{:S(2)}) async-start(), calls=%async_computation.5 | async-start | bytes 10027008 | tf_op jit(solution)/shard_map/all_gather | solution.py:39
  140.2 135.2 %copy-start.12 = (bf16[768,2048]{1,0:T(8,128)(2,1)S(1)}, bf16[768,2048]{1,0:T(8,128)(2,1)}, u32[]{:S(2)}) copy-start(bf16[768,2048]{1,0:T(8,128)(2,1)} %all-gather.6.cloned.1.call-done) | copy-start | bytes 9437188
  337.7 2.6 copy-start.10
Sparse Core Ops, SparseCore 0:
  55.1 47.0 all-gather.3
  107.5 32.6 all-gather.5
  141.9 126.5 all-gather.7
where the time goes:
time: 349 us
  waiting for transfers between devices  172 us (49%)
  blocking collectives  116 us (33%)
  matrix products  22.3 us (6%)
  between operations  13.5 us (4%)
  starting transfers between devices  12.4 us (4%)
  other arithmetic  8.34 us (2%)
  local copies, waits for them, and re-layouts  4.39 us (1%)
    all_gather x1, waiting for transfers between devices, turned_gather(): lax.all_gather(both, axis, axis=0, tiled=True)  128 us
    all_to_all x1, blocking collectives, summed_on_arrival(): pieces = lax.all_to_all(split_up(shard, dim, size), axis, 0, 0, tiled=True)  51.4 us
    all_to_all x1, blocking collectives, from_everyone(): lax.all_to_all(jnp.broadcast_to(shard[None], (size, *shard.shape)), axis,...  47.2 us
    all_gather x1, waiting for transfers between devices, per_device(): piece = lax.all_gather(normed, 'tp', axis=0, tiled=True)  31.3 us
    all_to_all x1, blocking collectives, per_device(): lax.all_to_all(mixed, 'tp', split_axis=0, concat_axis=1, tiled=True)  17.5 us
    all_gather x1, waiting for transfers between devices, per_device(): lax.all_gather(head_columns, 'tp', axis=0, tiled=True)  12.1 us
    ppermute x3, starting transfers between devices, passed_along(): lax.ppermute(value, axis, [(source, source + steps) for source in range(f...  12 us
    dot_general x1, matrix products, per_device(): jnp.dot(hidden, full_down, preferred_element_type=jnp.float32)  11 us
  transfers between devices with their start and end apart: 6, of which 3 were waited for; matrix products, arithmetic and copies ran while one was open for 2% of the time, Pallas kernels for 0%

commit v1 on v0

--- a/solution.py
+++ b/solution.py
@@ -7,6 +7,11 @@
 WINDOW = 128
 epsilon = 1e-06
 masked_value = -1e30
+
+
+def tiled_gather(x, axis, dim):
+    copies = jnp.concatenate([x] * lax.axis_size(axis), axis=dim)
+    return lax.all_to_all(copies, axis, dim, dim, tiled=True)
 
 
 def passed_along(value, axis, steps):
@@ -142,7 +147,7 @@
     full_gate, full_up, full_down = turned_gather(
         (gate_weight, up_weight, down_weight), "sp", (0, 0, 1)
     )
-    piece = lax.all_gather(normed, "tp", axis=0, tiled=True)
+    piece = tiled_gather(normed, "tp", 0)
     gate = jnp.dot(piece, full_gate, preferred_element_type=jnp.float32)
     upward = jnp.dot(piece, full_up, preferred_element_type=jnp.float32)
     hidden = (jax.nn.silu(gate) * upward).astype(jnp.bfloat16)

time: 349 us -> 312 us (0.89)
  waiting for transfers between devices: 172 us -> 91.8 us
  blocking collectives: 116 us -> 158 us
    all_gather x1, waiting for transfers between devices: 128 us -> 82.2 us  [turned_gather(): lax.all_gather(both, axis, axis=0, tiled=True)]
    all_to_all x0 -> x1, blocking collectives: none -> 41.4 us  [tiled_gather(): return lax.all_to_all(copies, axis, dim, dim, tiled=True)]
    all_gather x1 -> x0, waiting for transfers between devices: 31.3 us -> none  [per_device(): piece = lax.all_gather(normed, 'tp', axis=0, tiled=True)]
  transfers between devices with their start and end apart: 6 -> 5, of which waited for: 3 -> 2; matrix products, arithmetic and copies ran while one was open for 2% -> 4% of each run, Pallas kernels for 0% -> 0%
where the time goes in v1:
time: 312 us; the launch traced here: 311 us
  blocking collectives  158 us (51%)
  waiting for transfers between devices  91.8 us (29%)
  matrix products  21.4 us (7%)
  between operations  13.8 us (4%)
  starting transfers between devices  12.2 us (4%)
  other arithmetic  9.62 us (3%)
  local copies, waits for them, and re-layouts  4.12 us (1%)
    all_gather x1, waiting for transfers between devices, turned_gather(): lax.all_gather(both, axis, axis=0, tiled=True)  82.2 us
    all_to_all x1, blocking collectives, summed_on_arrival(): pieces = lax.all_to_all(split_up(shard, dim, size), axis, 0, 0, tiled=True)  51.4 us
    all_to_all x1, blocking collectives, from_everyone(): lax.all_to_all(jnp.broadcast_to(shard[None], (size, *shard.shape)), axis,...  47.2 us
    all_to_all x1, blocking collectives, tiled_gather(): return lax.all_to_all(copies, axis, dim, dim, tiled=True)  41.4 us
    all_to_all x1, blocking collectives, per_device(): lax.all_to_all(mixed, 'tp', split_axis=0, concat_axis=1, tiled=True)  18 us
    ppermute x3, starting transfers between devices, passed_along(): lax.ppermute(value, axis, [(source, source + steps) for source in range(f...  12.1 us
    dot_general x1, matrix products, per_device(): jnp.dot(hidden, full_down, preferred_element_type=jnp.float32)  11 us
    all_gather x1, waiting for transfers between devices, per_device(): lax.all_gather(head_columns, 'tp', axis=0, tiled=True)  9.57 us
  transfers between devices with their start and end apart: 5, of which 2 were waited for; matrix products, arithmetic and copies ran while one was open for 4% of the time, Pallas kernels for 0%

profile of v1, /device:TPU:33, one launch (start us, length us, event | category | flops | bytes accessed | tf_op | source)
XLA Modules:
  0.0 310.9 jit_solution(17891927789715655548)
XLA Ops:
  6.6 1.0 copy.40
  7.7 47.2 %all_to_all.38 = bf16[16,128,128]{1,2,0:T(8,128)(2,1)} all-to-all(bf16[16,128,128]{1,2,0:T(8,128)(2,1)S(1)} %broadcast_in_dim.16), channel_id=1, replica_groups=mesh['grp'=2,'sp'=16,'tp'=8] {'sp'}, dimensions={0} | all-to-all | bytes 1048576 | tf_op jit(solution)/shard_map/all_to_all | solution.py:25
  55.0 1.1 copy.41
  56.1 1.1 copy.42
  57.2 1.8 pad_maximum_fusion
  59.1 5.3 %collective-permute-start.1 = (s32[128]{0:T(128)S(1)}, s32[128]{0:T(128)S(1)}, u32[]{:S(2)}, u32[]{:S(2)}) collective-permute-start(s32[128]{0:T(128)S(1)} %slice.49), channel_id=1, source_target_pairs={{0,8},{8,16},{16,24},{24,32},{32,40},{40,48},{48,56},{56,64},{64,7... | collective-permute-start | bytes 1544 | tf_op jit(solution)/shard_map/ppermute | solution.py:20
  64.4 2.2 collective-permute-start
  66.6 4.6 %collective-permute-start.2 = (bf16[128,64]{0,1:T(8,128)(2,1)S(1)}, bf16[128,64]{0,1:T(8,128)(2,1)S(1)}, u32[]{:S(2)}, u32[]{:S(2)}) collective-permute-start(bf16[128,64]{0,1:T(8,128)(2,1)S(1)} %slice.52), channel_id=1, source_target_pairs={{0,8},{8,16},{16,24},{24,32},{32,40},{40,48},{48,56},{56,64},{64,7... | collective-permute-start | bytes 49160 | tf_op jit(solution)/shard_map/ppermute | solution.py:20
  71.6 1.0 fusion.30
  72.6 0.5 fusion.48
  73.2 0.2 fusion.7
  73.5 0.4 fusion.13
  73.9 0.4 copy.48
  74.5 18.0 %all_to_all.39 = bf16[8,96,128]{2,1,0:T(8,128)(2,1)S(1)} all-to-all(bf16[8,96,128]{2,1,0:T(8,128)(2,1)S(1)} %reshape.173), channel_id=1, replica_groups=mesh['grp'=2,'sp'=16,'tp'=8] {'tp'}, dimensions={0} | all-to-all | bytes 393216 | tf_op jit(solution)/shard_map/all_to_all | solution.py:138
  92.5 9.6 %all-gather.3.cloned.1.call-done = bf16[1024,2048]{0,1:T(8,128)(2,1)} async-done(((bf16[128,2048]{0,1:T(8,128)(2,1)}), bf16[1024,2048]{0,1:T(8,128)(2,1)}) %all-gather.3.cloned.1.call-update) | async-done | bytes 4194320 | tf_op jit(solution)/shard_map/all_gather | solution.py:141
  102.0 3.6 %convolution_convert_fusion.1 = bf16[96,2048]{1,0:T(8,128)(2,1)S(1)} fusion(bf16[1024,2048]{0,1:T(8,128)(2,1)} %all-gather.3.cloned.1.call-done, bf16[8,96,128]{2,1,0:T(8,128)(2,1)S(1)} %all_to_all.39), kind=kOutput, calls=%fused_computation.7 | convolution fusion | flops 402849792 | bytes 4784128 | tf_op jit(solution)/shard_map/dot_general | solution.py:139
  107.6 41.4 %all_to_all.40 = bf16[8,96,2048]{2,1,0:T(8,128)(2,1)S(1)} all-to-all(bf16[8,96,2048]{2,1,0:T(8,128)(2,1)S(1)} %bitcast.86), channel_id=1, replica_groups=mesh['grp'=2,'sp'=16,'tp'=8] {'tp'}, dimensions={0} | all-to-all | bytes 6291456 | tf_op jit(solution)/shard_map/all_to_all | solution.py:14
  149.0 82.2 %all-gather.5.cloned.1.call-done = bf16[2048,2304]{0,1:T(8,128)(2,1)} async-done(((bf16[128,2304]{0,1:T(8,128)(2,1)}), bf16[2048,2304]{0,1:T(8,128)(2,1)}) %all-gather.5.cloned.1.call-update) | async-done | bytes 9437200 | tf_op jit(solution)/shard_map/all_gather | solution.py:44
  231.2 6.0 %fusion.3 = f32[768,768]{1,0:T(8,128)} fusion(bf16[768,2048]{1,0:T(8,128)(2,1)S(1)} %bitcast.87, bf16[2048,2304]{0,1:T(8,128)(2,1)} %all-gather.5.cloned.1.call-done), kind=kOutput, calls=%fused_computation.4 | convolution fusion | flops 2415919104 | bytes 8650752 | tf_op jit(solution)/shard_map/dot_general | solution.py:151
  237.1 11.0 %convolution_convert_fusion = bf16[768,2048]{1,0:T(8,128)(2,1)} fusion(bf16[2048,2304]{0,1:T(8,128)(2,1)} %all-gather.5.cloned.1.call-done, f32[768,768]{1,0:T(8,128)} %fusion.3, bf16[768,2048]{1,0:T(8,128)(2,1)S(1)} %bitcast.88), kind=kOutput, calls=%fused_computation | convolution fusion | flops 4836950016 | bytes 14942208 | tf_op jit(solution)/shard_map/dot_general | solution.py:156
  248.1 51.4 %all_to_all.41 = bf16[8,96,2048]{2,1,0:T(8,128)(2,1)S(1)} all-to-all(bf16[8,96,2048]{2,1,0:T(8,128)(2,1)} %bitcast.89), channel_id=1, replica_groups=mesh['grp'=2,'sp'=16,'tp'=8] {'tp'}, dimensions={0} | all-to-all | bytes 6291456 | tf_op jit(solution)/shard_map/all_to_all | solution.py:60
  299.5 1.4 reduce_sum.54
  300.9 1.2 fusion.18
  302.1 2.0 fusion.24
  (58 shorter events, 2.9 us)
Async XLA Ops:
  6.5 52.5 %copy-start.5 = (s32[768]{0:T(1024)S(1)}, s32[768]{0:T(1024)}, u32[]{:S(2)}) copy-start(s32[768]{0:T(1024)} %param.16) | copy-start | bytes 9220
  6.5 57.8 %copy-start.2 = (bf16[768,64]{0,1:T(8,128)(2,1)S(1)}, bf16[768,64]{0,1:T(8,128)(2,1)}, u32[]{:S(2)}) copy-start(bf16[768,64]{0,1:T(8,128)(2,1)} %param.15) | copy-start | bytes 294916
  6.6 60.1 %copy-start.1 = (bf16[768,64]{0,1:T(8,128)(2,1)S(1)}, bf16[768,64]{0,1:T(8,128)(2,1)}, u32[]{:S(2)}) copy-start(bf16[768,64]{0,1:T(8,128)(2,1)} %param.14) | copy-start | bytes 294916
  6.6 64.8 %copy-start.4 = (bf16[768,128]{1,0:T(8,128)(2,1)S(1)}, bf16[768,128]{1,0:T(8,128)(2,1)}, u32[]{:S(2)}) copy-start(bf16[768,128]{1,0:T(8,128)(2,1)} %param.13) | copy-start | bytes 589828
  6.6 95.5 %all-gather.3.cloned.1.call-start = ((), (), s32[]{:S(2)}) async-start(), calls=%async_computation.4 | async-start | bytes 4718592 | tf_op jit(solution)/shard_map/all_gather | solution.py:141
  54.9 176.2 %all-gather.5.cloned.1.call-start = ((), (), s32[]{:S(2)}) async-start(), calls=%async_computation.5 | async-start | bytes 10027008 | tf_op jit(solution)/shard_map/all_gather | solution.py:44
  57.2 15.9 %copy-start.8 = (f32[2]{0:T(128)S(1)}, f32[2]{0:T(128)}, u32[]{:S(2)}) copy-start(f32[2]{0:T(128)} %param.17) | copy-start | bytes 28
  59.1 12.4 %collective-permute-start.1 = (s32[128]{0:T(128)S(1)}, s32[128]{0:T(128)S(1)}, u32[]{:S(2)}, u32[]{:S(2)}) collective-permute-start(s32[128]{0:T(128)S(1)} %slice.49), channel_id=1, source_target_pairs={{0,8},{8,16},{16,24},{24,32},{32,40},{40,48},{48,56},{56,64},{64,7... | collective-permute-start | bytes 1544 | tf_op jit(solution)/shard_map/ppermute | solution.py:20
  64.4 8.2 %collective-permute-start = (bf16[128,64]{0,1:T(8,128)(2,1)S(1)}, bf16[128,64]{0,1:T(8,128)(2,1)S(1)}, u32[]{:S(2)}, u32[]{:S(2)}) collective-permute-start(bf16[128,64]{0,1:T(8,128)(2,1)S(1)} %slice.45), channel_id=1, source_target_pairs={{0,8},{8,16},{16,24},{24,32},{32,40},{40,48},{48,56},{56,64},{64,7... | collective-permute-start | bytes 49160 | tf_op jit(solution)/shard_map/ppermute | solution.py:20
  66.6 5.9 %collective-permute-start.2 = (bf16[128,64]{0,1:T(8,128)(2,1)S(1)}, bf16[128,64]{0,1:T(8,128)(2,1)S(1)}, u32[]{:S(2)}, u32[]{:S(2)}) collective-permute-start(bf16[128,64]{0,1:T(8,128)(2,1)S(1)} %slice.52), channel_id=1, source_target_pairs={{0,8},{8,16},{16,24},{24,32},{32,40},{40,48},{48,56},{56,64},{64,7... | collective-permute-start | bytes 49160 | tf_op jit(solution)/shard_map/ppermute | solution.py:20
  74.3 31.6 %copy-start.3 = (bf16[96,2048]{1,0:T(8,128)(2,1)S(1)}, bf16[96,2048]{1,0:T(8,128)(2,1)}, u32[]{:S(2)}) copy-start(bf16[96,2048]{1,0:T(8,128)(2,1)} %param.19) | copy-start | bytes 1179652
  74.3 31.6 %copy-start.6 = (f32[2048]{0:T(1024)S(1)}, f32[2048]{0:T(1024)}, u32[]{:S(2)}) copy-start(f32[2048]{0:T(1024)} %param.20) | copy-start | bytes 24580
  92.5 13.8 %copy-start = (f32[2048]{0:T(1024)S(1)}, f32[2048]{0:T(1024)}, u32[]{:S(2)}) copy-start(f32[2048]{0:T(1024)} %param.21) | copy-start | bytes 24580
  299.5 2.6 copy-start.7
Sparse Core Ops, SparseCore 0:
  55.1 46.9 all-gather.2
  103.8 127.3 all-gather.4
